TPU v7x, 512 devices: a whole 4x4x16 slice. The times are simulated.
512 devices in a mesh: sp: 32 (over z, core), tp: 16 (over y, x).
Axes of the slice: x: 4, y: 4, z: 16, core: 2. Of those that a mesh axis runs over, the one named last changes fastest.
Arguments:
- residual: bfloat16 [8192, 2048], P('sp'), may hold values from -6 to 6
- queries: bfloat16 [8192, 16, 128], P('sp', 'tp'), may hold values from -256 to 256
- key_vectors: bfloat16 [8192, 16, 128], P('sp', 'tp'), may hold values from -5.3 to 5.3
- value_rows: bfloat16 [8192, 16, 128], P('sp', 'tp'), may hold values from -6 to 6
- head_lambda: float32 [16], P('tp'), may hold values from 0.3 to 0.8
- head_gain: float32 [128], replicated, may hold values from 0.1 to 1.9
- out_weight: bfloat16 [2048, 2048], P('tp'), may hold values from -0.125 to 0.125
- ffn_gain: float32 [2048], replicated, may hold values from 0.1 to 1.9
- expert_gate: bfloat16 [32, 2048, 4096], P('sp', None, 'tp'), may hold values from -0.125 to 0.125
- expert_up: bfloat16 [32, 2048, 4096], P('sp', None, 'tp'), may hold values from -0.125 to 0.125
- expert_down: bfloat16 [32, 4096, 2048], P('sp', None, 'tp'), may hold values from -0.09375 to 0.09375
- routing: int32 [8192, 2], P('sp'), may hold values from 0 to 31, as said below
- route_weight: float32 [8192, 2], P('sp'), may hold values from 0.1 to 0.9
Outputs:
- layer_out: bfloat16 [8192, 2048], P('sp')
Inputs may be any that keep to these rules, and one draw needn't show every extreme that they name: `routing`: each row names two different experts of one group of 8 consecutive experts. In each aligned block of 256 rows no expert is named by more than 32 rows, and in every block some expert is named by exactly 32 rows.
All inputs are finite; a program needn't handle non-finite values.
Results may differ from a plain program's by a relative error of at most 0.015.
Values may be sent and summed in bfloat16 or wider, within the bound.
No kernel may reach another device: no remote copies, remote signals or barrier semaphores. Data moves between devices by JAX's collectives and lax.ppermute only.
A program may use at most 64 MiB of HBM per device.

v0:
```python
import math
import jax
import jax.numpy as jnp
from jax import lax
from jax.sharding import PartitionSpec as P

GROUPS = 4
norm_eps = 1e-06


def sent_together(arrays, axis, dim, along):
    ends, at = ([], 0)
    for a in arrays[:-1]:
        at += a.shape[along]
        ends.append(at)
    both = jnp.concatenate(arrays, axis=along)
    return tuple(jnp.split(lax.all_gather(both, axis, axis=dim, tiled=True), ends, axis=along))


def in_blocks(array, dim, peers):
    before, after = (array.shape[:dim], array.shape[dim + 1 :])
    return jnp.moveaxis(array.reshape(*before, peers, -1, *after), dim, 0)


def sum_at_owner(array, axis, dim):
    parts = in_blocks(array, dim, lax.axis_size(axis))
    arrived = lax.all_to_all(parts, axis, split_axis=0, concat_axis=0, tiled=True)
    return arrived.astype(jnp.float32).sum(axis=0)


def padded_to(lines, peers):
    spare = -len(lines) % peers
    return jnp.pad(lines, [(0, spare)] + [(0, 0)] * (lines.ndim - 1))


def from_everyone(array, axis):
    peers = lax.axis_size(axis)
    return lax.all_to_all(
        jnp.broadcast_to(array[None], (peers, *array.shape)), axis, 0, 0, tiled=True
    )


def laid_out(parts, dim):
    parts = jnp.moveaxis(parts, 0, dim)
    dims = parts.shape
    return parts.reshape(*dims[:dim], dims[dim] * dims[dim + 1], *dims[dim + 2 :])


def collect(array, axis, dim):
    parts = from_everyone(array, axis)
    return laid_out(parts, dim)


def sum_by_parts(array, axes):
    lines = array.reshape(-1, array.shape[-1])
    own = sum_at_owner(padded_to(lines, lax.axis_size(axes)), axes, 0)
    whole = collect(own.astype(jnp.bfloat16), axes, 0)
    return whole[: len(lines)].reshape(array.shape).astype(jnp.float32)


def online_update(running, query_part, key_part, value_part, query_pos, key_pos, score_scale):
    highest, totals, accum = running
    scores = (
        jnp.einsum("qhd,khd->hqk", query_part, key_part, preferred_element_type=jnp.float32)
        * score_scale
    )
    scores = jnp.where(key_pos[None, None, :] <= query_pos[None, :, None], scores, -jnp.inf)
    new_high = jnp.maximum(highest, jnp.max(scores, axis=-1))
    shrink = jnp.exp(highest - new_high)
    weights = jnp.exp(scores - new_high[:, :, None])
    totals = shrink * totals + jnp.sum(weights, axis=-1)
    blended = jnp.einsum(
        "hqk,khe->qhe", weights.astype(jnp.bfloat16), value_part, preferred_element_type=jnp.float32
    )
    accum = jnp.transpose(shrink)[:, :, None] * accum + blended
    return (new_high, totals, accum)


def shards(
    residual,
    queries,
    key_vectors,
    value_rows,
    head_lambda,
    head_gain,
    out_weight,
    ffn_gain,
    expert_gate,
    expert_up,
    expert_down,
    routing,
    route_weight,
):
    tok_count = queries.shape[0]
    local_heads = queries.shape[1]
    half_width = queries.shape[2] // 2
    value_width = value_rows.shape[2]
    score_scale = half_width ** (-0.5)
    query_pos = lax.axis_index("sp") * tok_count + jnp.arange(tok_count, dtype=jnp.int32)
    last_query = query_pos[-1]
    first_half = queries[:, :, :half_width]
    second_half = queries[:, :, half_width:]
    start_high = jnp.full((local_heads, tok_count), -1e30, jnp.float32)
    start_total = jnp.zeros((local_heads, tok_count), jnp.float32)
    start_accum = jnp.zeros((tok_count, local_heads, value_width), jnp.float32)
    empty_state = (start_high, start_total, start_accum)
    running = (empty_state, empty_state)
    key_piece, value_piece = sent_together((key_vectors, value_rows), "sp", 0, 1)
    piece_len = key_piece.shape[0]
    block_len = math.gcd(piece_len, 512)
    block_count = piece_len // block_len
    key_blocks = key_piece.reshape(block_count, block_len, local_heads, 2 * half_width)
    value_blocks = value_piece.reshape(block_count, block_len, local_heads, value_width)

    def visit(current, stacked):
        block_index, key_block, value_block = stacked
        block_first = block_index * block_len
        key_pos = block_first + jnp.arange(block_len, dtype=jnp.int32)

        def compute(inside):
            first_state = online_update(
                inside[0],
                first_half,
                key_block[:, :, :half_width],
                value_block,
                query_pos,
                key_pos,
                score_scale,
            )
            second_state = online_update(
                inside[1],
                second_half,
                key_block[:, :, half_width:],
                value_block,
                query_pos,
                key_pos,
                score_scale,
            )
            return (first_state, second_state)

        return (lax.cond(block_first <= last_query, compute, lambda inside: inside, current), None)

    running, _ = lax.scan(
        visit, running, (jnp.arange(block_count, dtype=jnp.int32), key_blocks, value_blocks)
    )
    first_state, second_state = running
    first_out = first_state[2] / jnp.transpose(first_state[1])[:, :, None]
    second_out = second_state[2] / jnp.transpose(second_state[1])[:, :, None]
    combined = first_out - head_lambda[None, :, None] * second_out
    normed_heads = (
        combined
        * lax.rsqrt(jnp.mean(combined * combined, axis=-1, keepdims=True) + norm_eps)
        * head_gain
    )
    attended = normed_heads.astype(jnp.bfloat16).reshape(tok_count, local_heads * value_width)
    partial_proj = jnp.dot(attended, out_weight, preferred_element_type=jnp.float32)
    projected = sum_by_parts(partial_proj.astype(jnp.bfloat16), "tp")
    stream = residual.astype(jnp.float32) + projected
    block_normed = (
        stream * lax.rsqrt(jnp.mean(stream * stream, axis=-1, keepdims=True) + norm_eps) * ffn_gain
    ).astype(jnp.bfloat16)
    expert_count = lax.axis_size("sp")
    tp_count = lax.axis_size("tp")
    per_group = expert_count // GROUPS
    capacity = tok_count // per_group
    top_count = routing.shape[1]
    model_width = block_normed.shape[1]
    flat_routes = routing.reshape(-1)
    route_count = flat_routes.shape[0]
    onehot = (flat_routes[:, None] == jnp.arange(expert_count, dtype=jnp.int32)[None, :]).astype(
        jnp.int32
    )
    earlier = jnp.cumsum(onehot, axis=0) - onehot
    position = jnp.sum(earlier * onehot, axis=1)
    slot_index = flat_routes * capacity + position
    slot_token = (
        jnp.full((expert_count * capacity,), tok_count, jnp.int32)
        .at[slot_index]
        .set(jnp.arange(route_count, dtype=jnp.int32) // top_count)
    )
    slot_table = slot_token.reshape(expert_count, capacity)
    slice_width = model_width // tp_count
    own_columns = lax.dynamic_slice_in_dim(
        block_normed, lax.axis_index("tp") * slice_width, slice_width, 1
    )
    outgoing = jnp.take(own_columns, slot_table, axis=0, mode="fill", fill_value=0)
    landed = lax.all_to_all(outgoing, "sp", split_axis=0, concat_axis=0, tiled=True)
    arrived = collect(landed, "tp", 2)
    expert_rows = arrived.reshape(-1, model_width)
    gate_part = jnp.dot(expert_rows, expert_gate[0], preferred_element_type=jnp.float32)
    up_part = jnp.dot(expert_rows, expert_up[0], preferred_element_type=jnp.float32)
    inner_act = (jax.nn.silu(gate_part) * up_part).astype(jnp.bfloat16)
    down_width = expert_down.shape[2]
    weight_rows = expert_down[0]
    expert_sum = jnp.dot(
        lax.all_gather(inner_act, "tp", axis=1, tiled=True),
        weight_rows,
        preferred_element_type=jnp.float32,
    )
    expert_out = expert_sum.astype(jnp.bfloat16).reshape(expert_count, capacity, down_width)
    returned = lax.all_to_all(expert_out, "sp", split_axis=0, concat_axis=0, tiled=True)
    per_route = returned.reshape(expert_count * capacity, down_width)[slot_index]
    weighted = per_route.astype(jnp.float32) * route_weight.reshape(-1)[:, None]
    token_sum = jnp.sum(weighted.reshape(tok_count, top_count, down_width), axis=1)
    moe_rows = collect(token_sum.astype(jnp.bfloat16), "tp", 1).astype(token_sum.dtype)
    return (stream + moe_rows).astype(jnp.bfloat16)


def solution(mesh):
    in_specs = (
        P("sp", None),
        P("sp", "tp", None),
        P("sp", "tp", None),
        P("sp", "tp", None),
        P("tp"),
        P(),
        P("tp", None),
        P(),
        P("sp", None, "tp"),
        P("sp", None, "tp"),
        P("sp", None, "tp"),
        P("sp", None),
        P("sp", None),
    )
    out_specs = P("sp", None)
    return jax.shard_map(shards, mesh=mesh, in_specs=in_specs, out_specs=out_specs, check_vma=False)
```

profile of v0, /device:TPU:1, one launch (start us, length us, event | category | flops | bytes accessed | tf_op | source)
XLA Modules:
  0.0 460.8 jit_solution(17257785034887943455)
XLA Ops:
  6.5 1.6 pad_maximum_fusion
  8.9 1.0 fusion.59
  10.7 78.0 %all-gather.3.cloned.1.call-done = bf16[8192,2,128]{2,0,1:T(8,128)(2,1)} async-done(((bf16[256,2,128]{2,0,1:T(8,128)(2,1)}), bf16[8192,2,128]{2,0,1:T(8,128)(2,1)}) %all-gather.3.cloned.1.call-update) | async-done | bytes 4194320 | tf_op jit(solution)/shard_map/all_gather | solution.py:17
  88.7 3.8 fusion.58
  92.6 33.3 %while.21 = (s32[]{:T(128)}, f32[1,256]{1,0:T(1,128)S(1)}, f32[1,256]{1,0:T(1,128)S(1)}, f32[256,1,128]{0,2,1:T(8,128)S(1)}, f32[1,256]{1,0:T(1,128)S(1)}, /*ind...) while((s32[]{:T(128)}, f32[1,256]{1,0:T(1,128)S(1)}, ...), condition=%wide.region_7.8_spmd.clone, body=%wide.region_0.7_spmd.clone.sunk | while | flops 102893312 | bytes 4570543 | solution.py:143
  94.5 2.4 conditional.3
  94.5 0.9 dynamic-slice_bitcast_fusion
  126.0 2.5 convolution_convert_fusion
  128.6 6.5 %all-to-all-start = ((bf16[16,16,2048]{2,1,0:T(8,128)(2,1)}), bf16[16,16,2048]{2,1,0:T(8,128)(2,1)S(1)}, u32[]{:S(2)}, u32[]{:S(2)}) async-start(bf16[16,16,2048]{2,1,0:T(8,128)(2,1)} %bitcast.29), calls=%async_computation | async-start | bytes 2097152 | tf_op jit(solution)/shard_map/all_to_all | solution.py:27
  135.6 1.2 reduce-window.6
  137.4 14.1 %all-to-all-done = bf16[16,16,2048]{2,1,0:T(8,128)(2,1)S(1)} async-done(((bf16[16,16,2048]{2,1,0:T(8,128)(2,1)}), bf16[16,16,2048]{2,1,0:T(8,128)(2,1)S(1)}, u32[]{:S(2)}, u32[]{:S(2)}) %all-to-all-start) | async-done | bytes 1048608 | tf_op jit(solution)/shard_map/all_to_all | solution.py:27
  151.7 1.1 broadcast_in_dim.38
  152.8 4.5 all-to-all-start.1
  157.4 2.4 scatter_custom_fusion
  160.0 0.8 dynamic-slice
  160.8 12.4 %all-to-all-done.1 = bf16[16,16,2048]{2,1,0:T(8,128)(2,1)S(1)} async-done(((bf16[16,16,2048]{2,1,0:T(8,128)(2,1)}), bf16[16,16,2048]{2,1,0:T(8,128)(2,1)S(1)}, u32[]{:S(2)}, u32[]{:S(2)}) %all-to-all-start.1) | async-done | bytes 1048608 | tf_op jit(solution)/shard_map/all_to_all | solution.py:38
  173.7 3.2 gather_fusion
  177.2 65.0 %all_to_all.30 = bf16[32,32,128]{2,1,0:T(8,128)(2,1)S(1)} all-to-all(bf16[32,32,128]{2,1,0:T(8,128)(2,1)S(1)} %broadcast_select_fusion), channel_id=1, replica_groups=mesh['sp'=32,'tp'=16] {'sp'}, dimensions={0} | all-to-all | bytes 524288 | tf_op jit(solution)/shard_map/all_to_all | solution.py:187
  242.1 0.8 broadcast_in_dim.42
  242.9 52.7 %all_to_all.31 = bf16[16,32,32,128]{3,2,1,0:T(8,128)(2,1)S(1)} all-to-all(bf16[16,32,32,128]{3,2,1,0:T(8,128)(2,1)S(1)} %broadcast_in_dim.42), channel_id=1, replica_groups=mesh['sp'=32,'tp'=16] {'tp'}, dimensions={0} | all-to-all | bytes 8388608 | tf_op jit(solution)/shard_map/all_to_all | solution.py:38
  295.6 4.9 %copy.34 = bf16[32,32,16,128]{3,2,1,0:T(8,128)(2,1)S(1)} copy(bf16[32,32,16,128]{3,1,0,2:T(8,128)(2,1)S(1)} %bitcast.139) | data formatting | bytes 8388608 | tf_op jit(solution)/shard_map/transpose | solution.py:44
  300.5 1.3 fusion.26
  301.8 2.1 fusion.34
  303.9 81.9 %all-gather.5.cloned.1.call-done = bf16[1024,4096]{1,0:T(8,128)(2,1)} async-done(((bf16[1024,256]{1,0:T(8,128)(2,1)}), bf16[1024,4096]{1,0:T(8,128)(2,1)}) %all-gather.5.cloned.1.call-update) | async-done | bytes 8388624 | tf_op jit(solution)/shard_map/all_gather | solution.py:196
  385.8 6.6 %convolution_convert_fusion.1 = bf16[1024,128]{1,0:T(8,128)(2,1)} fusion(bf16[1024,4096]{1,0:T(8,128)(2,1)} %all-gather.5.cloned.1.call-done, bf16[1,4096,128]{2,1,0:T(8,128)(2,1)} %param.27), kind=kOutput, calls=%fused_computation.53 | convolution fusion | flops 1073872896 | bytes 9699328 | tf_op jit(solution)/shard_map/dot_general | solution.py:195
  392.4 14.4 %all-to-all-start.4 = ((bf16[32,32,128]{2,1,0:T(8,128)(2,1)}), bf16[32,32,128]{2,1,0:T(8,128)(2,1)S(1)}, u32[]{:S(2)}, u32[]{:S(2)}) async-start(bf16[32,32,128]{2,1,0:T(8,128)(2,1)} %bitcast.151), calls=%async_computation.4 | async-start | bytes 524288 | tf_op jit(solution)/shard_map/all_to_all | solution.py:201
  406.8 0.8 copy.35
  407.6 21.5 %all-to-all-done.4 = bf16[32,32,128]{2,1,0:T(8,128)(2,1)S(1)} async-done(((bf16[32,32,128]{2,1,0:T(8,128)(2,1)}), bf16[32,32,128]{2,1,0:T(8,128)(2,1)S(1)}, u32[]{:S(2)}, u32[]{:S(2)}) %all-to-all-start.4) | async-done | bytes 262176 | tf_op jit(solution)/shard_map/all_to_all | solution.py:201
  429.1 1.3 gather_fusion.1
  430.4 1.3 fusion.40
  432.0 20.5 %all_to_all.32 = bf16[16,256,128]{2,1,0:T(8,128)(2,1)S(1)} all-to-all(bf16[16,256,128]{2,1,0:T(8,128)(2,1)S(1)} %broadcast_in_dim.43), channel_id=1, replica_groups=mesh['sp'=32,'tp'=16] {'tp'}, dimensions={0} | all-to-all | bytes 2097152 | tf_op jit(solution)/shard_map/all_to_all | solution.py:38
  452.5 1.5 fusion.30
  (131 shorter events, 14.6 us)
Async XLA Ops:
  6.5 294.0 %copy-start = (bf16[1,2048,256]{2,1,0:T(8,128)(2,1)S(1)}, bf16[1,2048,256]{2,1,0:T(8,128)(2,1)}, u32[]{:S(2)}) copy-start(bf16[1,2048,256]{2,1,0:T(8,128)(2,1)} %param.25) | copy-start | bytes 3145732
  6.5 82.2 %all-gather.3.cloned.1.call-start = ((), (), s32[]{:S(2)}) async-start(), calls=%async_computation.6 | async-start | bytes 4325376 | tf_op jit(solution)/shard_map/all_gather | solution.py:17
  92.6 33.4 %copy-start.4 = (f32[128]{0:T(128)S(1)}, f32[128]{0:T(128)}, u32[]{:S(2)}) copy-start(f32[128]{0:T(128)} %param.22) | copy-start | bytes 1540
  126.0 9.2 %copy-start.2 = (s32[256,2]{0,1:T(2,128)S(1)}, s32[256,2]{0,1:T(2,128)}, u32[]{:S(2)}) copy-start(s32[256,2]{0,1:T(2,128)} %param.28) | copy-start | bytes 6148
  128.6 23.0 %all-to-all-start = ((bf16[16,16,2048]{2,1,0:T(8,128)(2,1)}), bf16[16,16,2048]{2,1,0:T(8,128)(2,1)S(1)}, u32[]{:S(2)}, u32[]{:S(2)}) async-start(bf16[16,16,2048]{2,1,0:T(8,128)(2,1)} %bitcast.29), calls=%async_computation | async-start | bytes 2097152 | tf_op jit(solution)/shard_map/all_to_all | solution.py:27
  137.4 35.8 %copy-start.1 = (bf16[256,2048]{1,0:T(8,128)(2,1)S(1)}, bf16[256,2048]{1,0:T(8,128)(2,1)}, u32[]{:S(2)}) copy-start(bf16[256,2048]{1,0:T(8,128)(2,1)} %param.17) | copy-start | bytes 3145732
  152.8 20.4 %all-to-all-start.1 = ((bf16[16,16,2048]{2,1,0:T(8,128)(2,1)}), bf16[16,16,2048]{2,1,0:T(8,128)(2,1)S(1)}, u32[]{:S(2)}, u32[]{:S(2)}) async-start(bf16[16,16,2048]{2,1,0:T(8,128)(2,1)} %broadcast_in_dim.38), calls=%async_computation.1 | async-start | bytes 2097152 | tf_op jit(solution)/shard_map/all_to_all | solution.py:38
  157.3 228.5 %all-gather.5.cloned.1.call-start = ((), (), s32[]{:S(2)}) async-start(), calls=%async_computation.7 | async-start | bytes 8912896 | tf_op jit(solution)/shard_map/all_gather | solution.py:196
  300.5 1.3 copy-start.5
  303.9 102.9 %copy-start.3 = (f32[256,2]{0,1:T(2,128)S(1)}, f32[256,2]{0,1:T(2,128)}, u32[]{:S(2)}) copy-start(f32[256,2]{0,1:T(2,128)} %param.29) | copy-start | bytes 6148
  392.4 36.6 %all-to-all-start.4 = ((bf16[32,32,128]{2,1,0:T(8,128)(2,1)}), bf16[32,32,128]{2,1,0:T(8,128)(2,1)S(1)}, u32[]{:S(2)}, u32[]{:S(2)}) async-start(bf16[32,32,128]{2,1,0:T(8,128)(2,1)} %bitcast.151), calls=%async_computation.4 | async-start | bytes 524288 | tf_op jit(solution)/shard_map/all_to_all | solution.py:201
Sparse Core Ops, SparseCore 0:
  9.5 79.1 all-gather.2
  304.0 81.7 all-gather.4
where the time goes:
time: 462 us; the launch traced here: 461 us
  waiting for transfers between devices  208 us (45%)
  blocking collectives  138 us (30%)
  local copies, waits for them, and re-layouts  32.7 us (7%)
  starting transfers between devices  25.4 us (5%)
  loops' own time  21.5 us (5%)
  between operations  14.4 us (3%)
  matrix products  13.6 us (3%)
  other arithmetic  7.04 us (2%)
    all_gather x1, waiting for transfers between devices, shards(): lax.all_gather(inner_act, 'tp', axis=1, tiled=True)  81.9 us
    all_gather x1, waiting for transfers between devices, sent_together(): lax.all_gather(both, axis, axis=dim, tiled=True)  78 us
    all_to_all x2, blocking collectives, from_everyone(): lax.all_to_all(jnp.broadcast_to(array[None], (peers, *array.shape)), axis...  73.2 us
    all_to_all x1, blocking collectives, shards(): lax.all_to_all(outgoing, 'sp', split_axis=0, concat_axis=0, tiled=True)  65 us
    all_to_all x1, waiting for transfers between devices, shards(): lax.all_to_all(expert_out, 'sp', split_axis=0, concat_axis=0, tiled=True)  21.5 us
    another operation x1, loops' own time, shards(): lax.scan(visit, running, (jnp.arange(block_count, dtype=jnp.int32), key_b...  21.2 us
    all_to_all x1, starting transfers between devices, shards(): lax.all_to_all(expert_out, 'sp', split_axis=0, concat_axis=0, tiled=True)  14.4 us
    all_to_all x1, waiting for transfers between devices, sum_at_owner(): lax.all_to_all(parts, axis, split_axis=0, concat_axis=0, tiled=True)  14.1 us
  transfers between devices with their start and end apart: 5, of which 5 were waited for; matrix products, arithmetic and copies ran while one was open for 2% of the time, Pallas kernels for 0%

commit v1 on v0

--- a/solution.py
+++ b/solution.py
@@ -6,6 +6,31 @@
 
 GROUPS = 4
 norm_eps = 1e-06
+
+
+def change_levels_all(inputs):
+    device_axis = "tp"
+    ready = lax.axis_size(device_axis)
+    val = lax.axis_index(device_axis)
+    q_next, mat_out, current_arr = (ready, val, inputs.shape[1])
+    panels = [nth * q_next if src_i == 1 else nth for src_i, nth in enumerate(inputs.shape)]
+    u1 = jnp.zeros(panels, inputs.dtype)
+    piece_next = lax.dynamic_update_slice_in_dim(u1, inputs, mat_out * current_arr, axis=1)
+    r_now = oldest = inputs
+    for w in range(1, q_next // 2 + 1):
+        o_now = range(q_next)
+        state_next = map(lambda src_i: (src_i, (src_i + 1) % q_next), o_now)
+        r_now = lax.ppermute(r_now, device_axis, list(state_next))
+        piece_next = lax.dynamic_update_slice_in_dim(
+            piece_next, r_now, (mat_out - w) % q_next * current_arr, axis=1
+        )
+        if 2 * w < q_next:
+            p_next = map(lambda src_i: (src_i, (src_i - 1) % q_next), range(q_next))
+            oldest = lax.ppermute(oldest, device_axis, list(p_next))
+            piece_next = lax.dynamic_update_slice_in_dim(
+                piece_next, oldest, (mat_out + w) % q_next * current_arr, axis=1
+            )
+    return piece_next
 
 
 def sent_together(arrays, axis, dim, along):
@@ -193,9 +218,7 @@
     down_width = expert_down.shape[2]
     weight_rows = expert_down[0]
     expert_sum = jnp.dot(
-        lax.all_gather(inner_act, "tp", axis=1, tiled=True),
-        weight_rows,
-        preferred_element_type=jnp.float32,
+        change_levels_all(inner_act), weight_rows, preferred_element_type=jnp.float32
     )
     expert_out = expert_sum.astype(jnp.bfloat16).reshape(expert_count, capacity, down_width)
     returned = lax.all_to_all(expert_out, "sp", split_axis=0, concat_axis=0, tiled=True)

time: 462 us -> 534 us (1.16)
  starting transfers between devices: 25.4 us -> 96 us
  blocking collectives: 138 us -> 84 us
  local copies, waits for them, and re-layouts: 32.7 us -> 67.5 us
  waiting for transfers between devices: 208 us -> 228 us
    all_gather x1 -> x0, waiting for transfers between devices: 81.9 us -> none  [shards(): lax.all_gather(inner_act, 'tp', axis=1, tiled=True)]
    all_to_all x1 -> x2, waiting for transfers between devices: 12.4 us -> 74.9 us  [from_everyone(): lax.all_to_all(jnp.broadcast_to(array[None], (peers, *array.shape)), axis...]
    ppermute x0 -> x15, starting transfers between devices: none -> 62.3 us  [the longest x7 46.8 us: change_levels_all(): oldest = lax.ppermute(oldest, device_axis, list(p_next))]
    all_to_all x2 -> x1, blocking collectives: 73.2 us -> 19 us  [from_everyone(): lax.all_to_all(jnp.broadcast_to(array[None], (peers, *array.shape)), axis...]
    ppermute x0 -> x15, waiting for transfers between devices: none -> 39 us  [the longest x8 39 us: change_levels_all(): r_now = lax.ppermute(r_now, device_axis, list(state_next))]
    dynamic_update_slice x0 -> x15, local copies, waits for them, and re-layouts: none -> 24.8 us  [the longest x8 13.4 us: change_levels_all(): lax.dynamic_update_slice_in_dim(piece_next, r_now, (mat_out - w) % q_next...]
  transfers between devices with their start and end apart: 5 -> 20, of which waited for: 5 -> 11; matrix products, arithmetic and copies ran while one was open for 2% -> 6% of each run, Pallas kernels for 0% -> 0%
where the time goes in v1:
time: 534 us; the launch traced here: 532 us
  waiting for transfers between devices  228 us (43%)
  starting transfers between devices  96 us (18%)
  blocking collectives  84 us (16%)
  local copies, waits for them, and re-layouts  67.5 us (13%)
  loops' own time  21.3 us (4%)
  between operations  14.8 us (3%)
  matrix products  13.6 us (3%)
  other arithmetic  7.1 us (1%)
    all_gather x1, waiting for transfers between devices, sent_together(): lax.all_gather(both, axis, axis=dim, tiled=True)  78 us
    all_to_all x2, waiting for transfers between devices, from_everyone(): lax.all_to_all(jnp.broadcast_to(array[None], (peers, *array.shape)), axis...  74.9 us
    all_to_all x1, blocking collectives, shards(): lax.all_to_all(outgoing, 'sp', split_axis=0, concat_axis=0, tiled=True)  65 us
    ppermute x7, starting transfers between devices, change_levels_all(): oldest = lax.ppermute(oldest, device_axis, list(p_next))  46.8 us
    ppermute x8, waiting for transfers between devices, change_levels_all(): r_now = lax.ppermute(r_now, device_axis, list(state_next))  39 us
    all_to_all x1, waiting for transfers between devices, shards(): lax.all_to_all(expert_out, 'sp', split_axis=0, concat_axis=0, tiled=True)  21.4 us
    another operation x1, loops' own time, shards(): lax.scan(visit, running, (jnp.arange(block_count, dtype=jnp.int32), key_b...  21 us
    all_to_all x1, blocking collectives, from_everyone(): lax.all_to_all(jnp.broadcast_to(array[None], (peers, *array.shape)), axis...  19 us
  transfers between devices with their start and end apart: 20, of which 11 were waited for; matrix products, arithmetic and copies ran while one was open for 6% of the time, Pallas kernels for 0%

profile of v1, /device:TPU:1, one launch (start us, length us, event | category | flops | bytes accessed | tf_op | source)
XLA Modules:
  0.0 531.8 jit_solution(4245987626586289316)
XLA Ops:
  10.7 78.0 %all-gather.2.cloned.1.call-done = bf16[8192,2,128]{2,0,1:T(8,128)(2,1)} async-done(((bf16[256,2,128]{2,0,1:T(8,128)(2,1)}), bf16[8192,2,128]{2,0,1:T(8,128)(2,1)}) %all-gather.2.cloned.1.call-update) | async-done | bytes 4194320 | tf_op jit(solution)/shard_map/all_gather | solution.py:42
  88.7 3.8 fusion.58
  92.6 33.1 %while.21 = (s32[]{:T(128)}, f32[1,256]{1,0:T(1,128)S(1)}, f32[1,256]{1,0:T(1,128)S(1)}, f32[256,1,128]{0,2,1:T(8,128)S(1)}, f32[1,256]{1,0:T(1,128)S(1)}, /*ind...) while((s32[]{:T(128)}, f32[1,256]{1,0:T(1,128)S(1)}, ...), condition=%wide.region_7.8_spmd.clone, body=%wide.region_0.7_spmd.clone.sunk | while | flops 102893312 | bytes 4570543 | solution.py:168
  125.9 2.6 convolution_convert_fusion
  128.5 6.5 %all-to-all-start = ((bf16[16,16,2048]{2,1,0:T(8,128)(2,1)}), bf16[16,16,2048]{2,1,0:T(8,128)(2,1)S(1)}, u32[]{:S(2)}, u32[]{:S(2)}) async-start(bf16[16,16,2048]{2,1,0:T(8,128)(2,1)} %bitcast.147), calls=%async_computation | async-start | bytes 2097152 | tf_op jit(solution)/shard_map/all_to_all | solution.py:52
  137.3 14.1 %all-to-all-done = bf16[16,16,2048]{2,1,0:T(8,128)(2,1)S(1)} async-done(((bf16[16,16,2048]{2,1,0:T(8,128)(2,1)}), bf16[16,16,2048]{2,1,0:T(8,128)(2,1)S(1)}, u32[]{:S(2)}, u32[]{:S(2)}) %all-to-all-start) | async-done | bytes 1048608 | tf_op jit(solution)/shard_map/all_to_all | solution.py:52
  152.7 4.5 all-to-all-start.1
  160.7 12.4 %all-to-all-done.1 = bf16[16,16,2048]{2,1,0:T(8,128)(2,1)S(1)} async-done(((bf16[16,16,2048]{2,1,0:T(8,128)(2,1)}), bf16[16,16,2048]{2,1,0:T(8,128)(2,1)S(1)}, u32[]{:S(2)}, u32[]{:S(2)}) %all-to-all-start.1) | async-done | bytes 1048608 | tf_op jit(solution)/shard_map/all_to_all | solution.py:63
  173.6 3.2 gather_fusion
  177.0 65.0 %all_to_all.30 = bf16[32,32,128]{2,1,0:T(8,128)(2,1)S(1)} all-to-all(bf16[32,32,128]{2,1,0:T(8,128)(2,1)S(1)} %broadcast_select_fusion), channel_id=1, replica_groups=mesh['sp'=32,'tp'=16] {'sp'}, dimensions={0} | all-to-all | bytes 524288 | tf_op jit(solution)/shard_map/all_to_all | solution.py:212
  242.0 2.8 broadcast_in_dim.70
  244.8 4.7 all-to-all-start.3
  249.6 62.5 %all-to-all-done.3 = bf16[16,32,32,128]{3,2,1,0:T(8,128)(2,1)} async-done(((bf16[16,32,32,128]{3,2,1,0:T(8,128)(2,1)}), bf16[16,32,32,128]{3,2,1,0:T(8,128)(2,1)}, u32[]{:S(2)}, u32[]{:S(2)}) %all-to-all-start.3) | async-done | bytes 4194336 | tf_op jit(solution)/shard_map/all_to_all | solution.py:63
  312.1 7.1 %copy.34 = bf16[32,32,16,128]{3,2,1,0:T(8,128)(2,1)S(1)} copy(bf16[32,32,16,128]{3,1,0,2:T(8,128)(2,1)} %bitcast.35) | data formatting | bytes 8388608 | tf_op jit(solution)/shard_map/transpose | solution.py:69
  320.5 4.3 broadcast_in_dim.41
  328.8 6.7 %collective-permute-start.1 = (bf16[1024,256]{1,0:T(8,128)(2,1)S(1)}, bf16[1024,256]{1,0:T(8,128)(2,1)S(1)}, u32[]{:S(2)}, u32[]{:S(2)}) collective-permute-start(bf16[1024,256]{1,0:T(8,128)(2,1)S(1)} %get-tuple-element.328), channel_id=1, source_target_pairs={{0,15},{1,0},{2,1},{3,2},{4,3},{5,4},{6,5},{7,6},{8,7},{9,8},{10,9... | collective-permute-start | bytes 1572872 | tf_op jit(solution)/shard_map/ppermute | solution.py:29
  335.5 8.6 %collective-permute-done = bf16[1024,256]{1,0:T(8,128)(2,1)S(1)} collective-permute-done((bf16[1024,256]{1,0:T(8,128)(2,1)S(1)}, bf16[1024,256]{1,0:T(8,128)(2,1)S(1)}, u32[]{:S(2)}, u32[]{:S(2)}) %collective-permute-start) | collective-permute-done | bytes 524320 | tf_op jit(solution)/shard_map/ppermute | solution.py:23
  346.1 6.7 %collective-permute-start.3 = (bf16[1024,256]{1,0:T(8,128)(2,1)S(1)}, bf16[1024,256]{1,0:T(8,128)(2,1)S(1)}, u32[]{:S(2)}, u32[]{:S(2)}) collective-permute-start(bf16[1024,256]{1,0:T(8,128)(2,1)S(1)} %collective-permute-done.1), channel_id=1, source_target_pairs={{0,15},{1,0},{2,1},{3,2},{4,3},{5,4},{6,5},{7,6},{8,7},{9,8},{10,9... | collective-permute-start | bytes 1572872 | tf_op jit(solution)/shard_map/ppermute | solution.py:29
  352.8 7.7 %collective-permute-done.2 = bf16[1024,256]{1,0:T(8,128)(2,1)S(1)} collective-permute-done((bf16[1024,256]{1,0:T(8,128)(2,1)S(1)}, bf16[1024,256]{1,0:T(8,128)(2,1)S(1)}, u32[]{:S(2)}, u32[]{:S(2)}) %collective-permute-start.2) | collective-permute-done | bytes 524320 | tf_op jit(solution)/shard_map/ppermute | solution.py:23
  362.4 6.7 %collective-permute-start.5 = (bf16[1024,256]{1,0:T(8,128)(2,1)S(1)}, bf16[1024,256]{1,0:T(8,128)(2,1)S(1)}, u32[]{:S(2)}, u32[]{:S(2)}) collective-permute-start(bf16[1024,256]{1,0:T(8,128)(2,1)S(1)} %collective-permute-done.3), channel_id=1, source_target_pairs={{0,15},{1,0},{2,1},{3,2},{4,3},{5,4},{6,5},{7,6},{8,7},{9,8},{10,9... | collective-permute-start | bytes 1572872 | tf_op jit(solution)/shard_map/ppermute | solution.py:29
  369.1 6.9 %collective-permute-done.4 = bf16[1024,256]{1,0:T(8,128)(2,1)S(1)} collective-permute-done((bf16[1024,256]{1,0:T(8,128)(2,1)S(1)}, bf16[1024,256]{1,0:T(8,128)(2,1)S(1)}, u32[]{:S(2)}, u32[]{:S(2)}) %collective-permute-start.4) | collective-permute-done | bytes 524320 | tf_op jit(solution)/shard_map/ppermute | solution.py:23
  378.7 6.7 %collective-permute-start.7 = (bf16[1024,256]{1,0:T(8,128)(2,1)S(1)}, bf16[1024,256]{1,0:T(8,128)(2,1)}, u32[]{:S(2)}, u32[]{:S(2)}) collective-permute-start(bf16[1024,256]{1,0:T(8,128)(2,1)S(1)} %collective-permute-done.5), channel_id=1, source_target_pairs={{0,15},{1,0},{2,1},{3,2},{4,3},{5,4},{6,5},{7,6},{8,7},{9,8},{10,9... | collective-permute-start | bytes 1572872 | tf_op jit(solution)/shard_map/ppermute | solution.py:29
  385.4 6.0 %collective-permute-done.6 = bf16[1024,256]{1,0:T(8,128)(2,1)S(1)} collective-permute-done((bf16[1024,256]{1,0:T(8,128)(2,1)S(1)}, bf16[1024,256]{1,0:T(8,128)(2,1)S(1)}, u32[]{:S(2)}, u32[]{:S(2)}) %collective-permute-start.6) | collective-permute-done | bytes 524320 | tf_op jit(solution)/shard_map/ppermute | solution.py:23
  393.4 6.7 %collective-permute-start.9 = (bf16[1024,256]{1,0:T(8,128)(2,1)}, bf16[1024,256]{1,0:T(8,128)(2,1)}, u32[]{:S(2)}, u32[]{:S(2)}) collective-permute-start(bf16[1024,256]{1,0:T(8,128)(2,1)} %collective-permute-done.7), channel_id=1, source_target_pairs={{0,15},{1,0},{2,1},{3,2},{4,3},{5,4},{6,5},{7,6},{8,7},{9,8},{10,9... | collective-permute-start | bytes 1572872 | tf_op jit(solution)/shard_map/ppermute | solution.py:29
  400.1 5.3 collective-permute-done.8
  413.4 6.7 %collective-permute-start.11 = (bf16[1024,256]{1,0:T(8,128)(2,1)}, bf16[1024,256]{1,0:T(8,128)(2,1)S(1)}, u32[]{:S(2)}, u32[]{:S(2)}) collective-permute-start(bf16[1024,256]{1,0:T(8,128)(2,1)} %collective-permute-done.9), channel_id=1, source_target_pairs={{0,15},{1,0},{2,1},{3,2},{4,3},{5,4},{6,5},{7,6},{8,7},{9,8},{10,9... | collective-permute-start | bytes 1572872 | tf_op jit(solution)/shard_map/ppermute | solution.py:29
  431.7 6.7 %collective-permute-start.13 = (bf16[1024,256]{1,0:T(8,128)(2,1)S(1)}, bf16[1024,256]{1,0:T(8,128)(2,1)S(1)}, u32[]{:S(2)}, u32[]{:S(2)}) collective-permute-start(bf16[1024,256]{1,0:T(8,128)(2,1)S(1)} %collective-permute-done.11), channel_id=1, source_target_pairs={{0,15},{1,0},{2,1},{3,2},{4,3},{5,4},{6,5},{7,6},{8,7},{9,8},{10,9... | collective-permute-start | bytes 1572872 | tf_op jit(solution)/shard_map/ppermute | solution.py:29
  449.0 4.6 collective-permute-done.14
  454.4 6.4 %convolution_convert_fusion.1 = bf16[1024,128]{1,0:T(8,128)(2,1)} fusion(bf16[1024,4096]{1,0:T(8,128)(2,1)} %constant_dynamic-update-slice_fusion, bf16[1,4096,128]{2,1,0:T(8,128)(2,1)S(1)} %copy-done.13), kind=kOutput, calls=%fused_computation.53 | convolution fusion | flops 1073872896 | bytes 9699328 | tf_op jit(solution)/shard_map/dot_general | solution.py:220
  460.8 17.9 %all-to-all-start.4 = ((bf16[32,32,128]{2,1,0:T(8,128)(2,1)}), bf16[32,32,128]{2,1,0:T(8,128)(2,1)S(1)}, u32[]{:S(2)}, u32[]{:S(2)}) async-start(bf16[32,32,128]{2,1,0:T(8,128)(2,1)} %bitcast.155), calls=%async_computation.4 | async-start | bytes 524288 | tf_op jit(solution)/shard_map/all_to_all | solution.py:224
  479.6 21.4 %all-to-all-done.4 = bf16[32,32,128]{2,1,0:T(8,128)(2,1)S(1)} async-done(((bf16[32,32,128]{2,1,0:T(8,128)(2,1)}), bf16[32,32,128]{2,1,0:T(8,128)(2,1)S(1)}, u32[]{:S(2)}, u32[]{:S(2)}) %all-to-all-start.4) | async-done | bytes 262176 | tf_op jit(solution)/shard_map/all_to_all | solution.py:224
  504.5 19.0 %all_to_all.31 = bf16[16,256,128]{2,1,0:T(8,128)(2,1)S(1)} all-to-all(bf16[16,256,128]{2,1,0:T(8,128)(2,1)S(1)} %broadcast_in_dim.71), channel_id=1, replica_groups=mesh['sp'=32,'tp'=16] {'tp'}, dimensions={0} | all-to-all | bytes 2097152 | tf_op jit(solution)/shard_map/all_to_all | solution.py:63
  (191 shorter events, 76.1 us)
Async XLA Ops:
  6.5 318.2 %copy-start = (bf16[1,2048,256]{2,1,0:T(8,128)(2,1)S(1)}, bf16[1,2048,256]{2,1,0:T(8,128)(2,1)}, u32[]{:S(2)}) copy-start(bf16[1,2048,256]{2,1,0:T(8,128)(2,1)} %param.26) | copy-start | bytes 3145732
  6.5 82.2 %all-gather.2.cloned.1.call-start = ((), (), s32[]{:S(2)}) async-start(), calls=%async_computation.6 | async-start | bytes 4325376 | tf_op jit(solution)/shard_map/all_gather | solution.py:42
  92.6 33.2 %copy-start.11 = (f32[128]{0:T(128)S(1)}, f32[128]{0:T(128)}, u32[]{:S(2)}) copy-start(f32[128]{0:T(128)} %param.22) | copy-start | bytes 1540
  92.6 42.4 %copy-start.9 = (s32[256,2]{0,1:T(2,128)S(1)}, s32[256,2]{0,1:T(2,128)}, u32[]{:S(2)}) copy-start(s32[256,2]{0,1:T(2,128)} %param.28) | copy-start | bytes 6148
  125.8 47.3 %copy-start.1 = (bf16[256,2048]{1,0:T(8,128)(2,1)S(1)}, bf16[256,2048]{1,0:T(8,128)(2,1)}, u32[]{:S(2)}) copy-start(bf16[256,2048]{1,0:T(8,128)(2,1)} %param.17) | copy-start | bytes 3145732
  128.5 23.0 %all-to-all-start = ((bf16[16,16,2048]{2,1,0:T(8,128)(2,1)}), bf16[16,16,2048]{2,1,0:T(8,128)(2,1)S(1)}, u32[]{:S(2)}, u32[]{:S(2)}) async-start(bf16[16,16,2048]{2,1,0:T(8,128)(2,1)} %bitcast.147), calls=%async_computation | async-start | bytes 2097152 | tf_op jit(solution)/shard_map/all_to_all | solution.py:52
  152.7 20.4 %all-to-all-start.1 = ((bf16[16,16,2048]{2,1,0:T(8,128)(2,1)}), bf16[16,16,2048]{2,1,0:T(8,128)(2,1)S(1)}, u32[]{:S(2)}, u32[]{:S(2)}) async-start(bf16[16,16,2048]{2,1,0:T(8,128)(2,1)} %broadcast_in_dim.40), calls=%async_computation.1 | async-start | bytes 2097152 | tf_op jit(solution)/shard_map/all_to_all | solution.py:63
  244.8 67.2 %all-to-all-start.3 = ((bf16[16,32,32,128]{3,2,1,0:T(8,128)(2,1)}), bf16[16,32,32,128]{3,2,1,0:T(8,128)(2,1)}, u32[]{:S(2)}, u32[]{:S(2)}) async-start(bf16[16,32,32,128]{3,2,1,0:T(8,128)(2,1)} %broadcast_in_dim.70), calls=%async_computation.3 | async-start | bytes 8388608 | tf_op jit(solution)/shard_map/all_to_all | solution.py:63
  326.9 17.2 %collective-permute-start = (bf16[1024,256]{1,0:T(8,128)(2,1)S(1)}, bf16[1024,256]{1,0:T(8,128)(2,1)S(1)}, u32[]{:S(2)}, u32[]{:S(2)}) collective-permute-start(bf16[1024,256]{1,0:T(8,128)(2,1)S(1)} %get-tuple-element.328), channel_id=1, source_target_pairs={{0,1},{1,2},{2,3},{3,4},{4,5},{5,6},{6,7},{7,8},{8,9},{9,10},{10,1... | collective-permute-start | bytes 1572872 | tf_op jit(solution)/shard_map/ppermute | solution.py:23
  328.8 17.2 %collective-permute-start.1 = (bf16[1024,256]{1,0:T(8,128)(2,1)S(1)}, bf16[1024,256]{1,0:T(8,128)(2,1)S(1)}, u32[]{:S(2)}, u32[]{:S(2)}) collective-permute-start(bf16[1024,256]{1,0:T(8,128)(2,1)S(1)} %get-tuple-element.328), channel_id=1, source_target_pairs={{0,15},{1,0},{2,1},{3,2},{4,3},{5,4},{6,5},{7,6},{8,7},{9,8},{10,9... | collective-permute-start | bytes 1572872 | tf_op jit(solution)/shard_map/ppermute | solution.py:29
  344.1 8.6 %copy-start.3 = (bf16[1024,256]{1,0:T(8,128)(2,1)}, bf16[1024,256]{1,0:T(8,128)(2,1)S(1)}, u32[]{:S(2)}) copy-start(bf16[1024,256]{1,0:T(8,128)(2,1)S(1)} %collective-permute-done) | copy-start | bytes 1572868
  344.1 16.4 %collective-permute-start.2 = (bf16[1024,256]{1,0:T(8,128)(2,1)S(1)}, bf16[1024,256]{1,0:T(8,128)(2,1)S(1)}, u32[]{:S(2)}, u32[]{:S(2)}) collective-permute-start(bf16[1024,256]{1,0:T(8,128)(2,1)S(1)} %collective-permute-done), channel_id=1, source_target_pairs={{0,1},{1,2},{2,3},{3,4},{4,5},{5,6},{6,7},{7,8},{8,9},{9,10},{10,1... | collective-permute-start | bytes 1572872 | tf_op jit(solution)/shard_map/ppermute | solution.py:23
  346.1 16.3 %copy-start.5 = (bf16[1024,256]{1,0:T(8,128)(2,1)}, bf16[1024,256]{1,0:T(8,128)(2,1)S(1)}, u32[]{:S(2)}) copy-start(bf16[1024,256]{1,0:T(8,128)(2,1)S(1)} %collective-permute-done.1) | copy-start | bytes 1572868
  346.1 16.3 %collective-permute-start.3 = (bf16[1024,256]{1,0:T(8,128)(2,1)S(1)}, bf16[1024,256]{1,0:T(8,128)(2,1)S(1)}, u32[]{:S(2)}, u32[]{:S(2)}) collective-permute-start(bf16[1024,256]{1,0:T(8,128)(2,1)S(1)} %collective-permute-done.1), channel_id=1, source_target_pairs={{0,15},{1,0},{2,1},{3,2},{4,3},{5,4},{6,5},{7,6},{8,7},{9,8},{10,9... | collective-permute-start | bytes 1572872 | tf_op jit(solution)/shard_map/ppermute | solution.py:29
  360.5 8.6 %copy-start.8 = (bf16[1024,256]{1,0:T(8,128)(2,1)}, bf16[1024,256]{1,0:T(8,128)(2,1)S(1)}, u32[]{:S(2)}) copy-start(bf16[1024,256]{1,0:T(8,128)(2,1)S(1)} %collective-permute-done.2) | copy-start | bytes 1572868
  360.5 15.5 %collective-permute-start.4 = (bf16[1024,256]{1,0:T(8,128)(2,1)S(1)}, bf16[1024,256]{1,0:T(8,128)(2,1)S(1)}, u32[]{:S(2)}, u32[]{:S(2)}) collective-permute-start(bf16[1024,256]{1,0:T(8,128)(2,1)S(1)} %collective-permute-done.2), channel_id=1, source_target_pairs={{0,1},{1,2},{2,3},{3,4},{4,5},{5,6},{6,7},{7,8},{8,9},{9,10},{10,1... | collective-permute-start | bytes 1572872 | tf_op jit(solution)/shard_map/ppermute | solution.py:23
  362.4 30.9 %copy-start.6 = (bf16[1024,256]{1,0:T(8,128)(2,1)}, bf16[1024,256]{1,0:T(8,128)(2,1)S(1)}, u32[]{:S(2)}) copy-start(bf16[1024,256]{1,0:T(8,128)(2,1)S(1)} %collective-permute-done.3) | copy-start | bytes 1572868
  362.4 16.3 %collective-permute-start.5 = (bf16[1024,256]{1,0:T(8,128)(2,1)S(1)}, bf16[1024,256]{1,0:T(8,128)(2,1)S(1)}, u32[]{:S(2)}, u32[]{:S(2)}) collective-permute-start(bf16[1024,256]{1,0:T(8,128)(2,1)S(1)} %collective-permute-done.3), channel_id=1, source_target_pairs={{0,15},{1,0},{2,1},{3,2},{4,3},{5,4},{6,5},{7,6},{8,7},{9,8},{10,9... | collective-permute-start | bytes 1572872 | tf_op jit(solution)/shard_map/ppermute | solution.py:29
  376.8 14.6 %collective-permute-start.6 = (bf16[1024,256]{1,0:T(8,128)(2,1)S(1)}, bf16[1024,256]{1,0:T(8,128)(2,1)S(1)}, u32[]{:S(2)}, u32[]{:S(2)}) collective-permute-start(bf16[1024,256]{1,0:T(8,128)(2,1)S(1)} %collective-permute-done.4), channel_id=1, source_target_pairs={{0,1},{1,2},{2,3},{3,4},{4,5},{5,6},{6,7},{7,8},{8,9},{9,10},{10,1... | collective-permute-start | bytes 1572872 | tf_op jit(solution)/shard_map/ppermute | solution.py:23
  378.7 12.7 %copy-start.4 = (bf16[1024,256]{1,0:T(8,128)(2,1)}, bf16[1024,256]{1,0:T(8,128)(2,1)S(1)}, u32[]{:S(2)}) copy-start(bf16[1024,256]{1,0:T(8,128)(2,1)S(1)} %collective-permute-done.5) | copy-start | bytes 1572868
  378.7 14.6 %collective-permute-start.7 = (bf16[1024,256]{1,0:T(8,128)(2,1)S(1)}, bf16[1024,256]{1,0:T(8,128)(2,1)}, u32[]{:S(2)}, u32[]{:S(2)}) collective-permute-start(bf16[1024,256]{1,0:T(8,128)(2,1)S(1)} %collective-permute-done.5), channel_id=1, source_target_pairs={{0,15},{1,0},{2,1},{3,2},{4,3},{5,4},{6,5},{7,6},{8,7},{9,8},{10,9... | collective-permute-start | bytes 1572872 | tf_op jit(solution)/shard_map/ppermute | solution.py:29
  391.4 8.6 %copy-start.7 = (bf16[1024,256]{1,0:T(8,128)(2,1)}, bf16[1024,256]{1,0:T(8,128)(2,1)S(1)}, u32[]{:S(2)}) copy-start(bf16[1024,256]{1,0:T(8,128)(2,1)S(1)} %collective-permute-done.6) | copy-start | bytes 1572868
  391.4 13.9 %collective-permute-start.8 = (bf16[1024,256]{1,0:T(8,128)(2,1)S(1)}, bf16[1024,256]{1,0:T(8,128)(2,1)}, u32[]{:S(2)}, u32[]{:S(2)}) collective-permute-start(bf16[1024,256]{1,0:T(8,128)(2,1)S(1)} %collective-permute-done.6), channel_id=1, source_target_pairs={{0,1},{1,2},{2,3},{3,4},{4,5},{5,6},{6,7},{7,8},{8,9},{9,10},{10,1... | collective-permute-start | bytes 1572872 | tf_op jit(solution)/shard_map/ppermute | solution.py:23
  393.4 20.0 %collective-permute-start.9 = (bf16[1024,256]{1,0:T(8,128)(2,1)}, bf16[1024,256]{1,0:T(8,128)(2,1)}, u32[]{:S(2)}, u32[]{:S(2)}) collective-permute-start(bf16[1024,256]{1,0:T(8,128)(2,1)} %collective-permute-done.7), channel_id=1, source_target_pairs={{0,15},{1,0},{2,1},{3,2},{4,3},{5,4},{6,5},{7,6},{8,7},{9,8},{10,9... | collective-permute-start | bytes 1572872 | tf_op jit(solution)/shard_map/ppermute | solution.py:29
  405.3 16.7 %collective-permute-start.10 = (bf16[1024,256]{1,0:T(8,128)(2,1)}, bf16[1024,256]{1,0:T(8,128)(2,1)}, u32[]{:S(2)}, u32[]{:S(2)}) collective-permute-start(bf16[1024,256]{1,0:T(8,128)(2,1)} %collective-permute-done.8), channel_id=1, source_target_pairs={{0,1},{1,2},{2,3},{3,4},{4,5},{5,6},{6,7},{7,8},{8,9},{9,10},{10,1... | collective-permute-start | bytes 1572872 | tf_op jit(solution)/shard_map/ppermute | solution.py:23
  407.5 46.9 %copy-start.13 = (bf16[1,4096,128]{2,1,0:T(8,128)(2,1)S(1)}, bf16[1,4096,128]{2,1,0:T(8,128)(2,1)}, u32[]{:S(2)}) copy-start(bf16[1,4096,128]{2,1,0:T(8,128)(2,1)} %param.27) | copy-start | bytes 3145732
  413.4 18.3 %collective-permute-start.11 = (bf16[1024,256]{1,0:T(8,128)(2,1)}, bf16[1024,256]{1,0:T(8,128)(2,1)S(1)}, u32[]{:S(2)}, u32[]{:S(2)}) collective-permute-start(bf16[1024,256]{1,0:T(8,128)(2,1)} %collective-permute-done.9), channel_id=1, source_target_pairs={{0,15},{1,0},{2,1},{3,2},{4,3},{5,4},{6,5},{7,6},{8,7},{9,8},{10,9... | collective-permute-start | bytes 1572872 | tf_op jit(solution)/shard_map/ppermute | solution.py:29
  422.0 18.3 %collective-permute-start.12 = (bf16[1024,256]{1,0:T(8,128)(2,1)}, bf16[1024,256]{1,0:T(8,128)(2,1)S(1)}, u32[]{:S(2)}, u32[]{:S(2)}) collective-permute-start(bf16[1024,256]{1,0:T(8,128)(2,1)} %collective-permute-done.10), channel_id=1, source_target_pairs={{0,1},{1,2},{2,3},{3,4},{4,5},{5,6},{6,7},{7,8},{8,9},{9,10},{10,1... | collective-permute-start | bytes 1572872 | tf_op jit(solution)/shard_map/ppermute | solution.py:23
  431.7 16.4 %collective-permute-start.13 = (bf16[1024,256]{1,0:T(8,128)(2,1)S(1)}, bf16[1024,256]{1,0:T(8,128)(2,1)S(1)}, u32[]{:S(2)}, u32[]{:S(2)}) collective-permute-start(bf16[1024,256]{1,0:T(8,128)(2,1)S(1)} %collective-permute-done.11), channel_id=1, source_target_pairs={{0,15},{1,0},{2,1},{3,2},{4,3},{5,4},{6,5},{7,6},{8,7},{9,8},{10,9... | collective-permute-start | bytes 1572872 | tf_op jit(solution)/shard_map/ppermute | solution.py:29
  440.3 13.2 %collective-permute-start.14 = (bf16[1024,256]{1,0:T(8,128)(2,1)S(1)}, bf16[1024,256]{1,0:T(8,128)(2,1)S(1)}, u32[]{:S(2)}, u32[]{:S(2)}) collective-permute-start(bf16[1024,256]{1,0:T(8,128)(2,1)S(1)} %collective-permute-done.12), channel_id=1, source_target_pairs={{0,1},{1,2},{2,3},{3,4},{4,5},{5,6},{6,7},{7,8},{8,9},{9,10},{10,1... | collective-permute-start | bytes 1572872 | tf_op jit(solution)/shard_map/ppermute | solution.py:23
  446.3 32.5 %copy-start.10 = (f32[256,2]{0,1:T(2,128)S(1)}, f32[256,2]{0,1:T(2,128)}, u32[]{:S(2)}) copy-start(f32[256,2]{0,1:T(2,128)} %param.29) | copy-start | bytes 6148
  460.8 40.2 %all-to-all-start.4 = ((bf16[32,32,128]{2,1,0:T(8,128)(2,1)}), bf16[32,32,128]{2,1,0:T(8,128)(2,1)S(1)}, u32[]{:S(2)}, u32[]{:S(2)}) async-start(bf16[32,32,128]{2,1,0:T(8,128)(2,1)} %bitcast.155), calls=%async_computation.4 | async-start | bytes 524288 | tf_op jit(solution)/shard_map/all_to_all | solution.py:224
  (2 other events, 7.9 us)
Sparse Core Ops, SparseCore 0:
  9.5 79.1 all-gather.1
